TPU v7x, 32 devices: a whole 2x2x4 slice. The times are simulated.
32 devices in a mesh: kv: 8 (over z, y), tp: 4 (over x, core).
Axes of the slice: x: 2, y: 2, z: 4, core: 2. Of those that a mesh axis runs over, the one named last changes fastest.
Arguments:
- tokens: bfloat16 [256, 4, 2048], P(None, None, ('kv', 'tp')), may hold values from -520 to 520
- input_norm_gain: bfloat16 [2048], replicated, may hold values from 0.099609375 to 1.8984375
- query_weight: bfloat16 [2048, 2048], P(None, 'kv'), may hold values from -0.125 to 0.125
- key_weight: bfloat16 [2048, 2048], P(None, 'kv'), may hold values from -0.125 to 0.125
- value_weight: bfloat16 [2048, 16, 128], P(None, 'kv', 'tp'), may hold values from -1.14904852 to 1.14904852
- output_gate_weight: bfloat16 [2048, 16, 128], P(None, 'kv', 'tp'), may hold values from -0.125 to 0.125
- strength_weight: bfloat16 [2048, 16], P(None, 'kv'), may hold values from -0.125 to 0.125
- decay_weight: bfloat16 [2048, 16], P(None, 'kv'), may hold values from -0.125 to 0.125
- head_decay_rate: float32 [16], P('kv'), may hold values from 0.005 to 1.5
- proposal_log_decay: float32 [256, 4, 16], P(None, None, 'kv'), may hold values from -0.69 to 0
- head_norm_gain: bfloat16 [128], P('tp'), may hold values from 0.099609375 to 1.8984375
- output_weight: bfloat16 [16, 128, 2048], P('kv', 'tp'), may hold values from -1.14904852 to 1.14904852
- output_norm_gain: bfloat16 [2048], P(('kv', 'tp')), may hold values from 0.099609375 to 1.8984375
- state: float32 [256, 16, 128, 128], P(None, 'kv', 'tp'), may hold values from -4.5961941 to 4.5961941
- previous_keys: bfloat16 [256, 4, 2048], P(None, None, 'kv'), may hold values from -6 to 6
- previous_values: bfloat16 [256, 4, 16, 128], P(None, None, 'kv', 'tp'), may hold values from -52 to 52
- previous_log_decay: float32 [256, 4, 16], P(None, None, 'kv'), may hold values from -0.7 to -0.02
- previous_strengths: float32 [256, 4, 16], P(None, None, 'kv'), may hold values from 0.1 to 0.9
- accepted: int32 [256], replicated, may hold values from 0 to 4
- parent: int32 [256, 4], replicated, may hold values from -1 to 2, as said below
Outputs:
- layer_out: bfloat16 [256, 4, 2048], P(None, None, ('kv', 'tp'))
- accepted_state: float32 [256, 16, 128, 128], P(None, 'kv', 'tp')
Inputs may be any that keep to these rules, and one draw needn't show every extreme that they name: parent[b, i] is -1 or a proposal index below i; -1 means that proposal i follows the accepted old proposals directly.
All inputs are finite; a program needn't handle non-finite values.
Results may differ from a plain program's by a relative error of at most 0.019.
Values may be sent and summed in bfloat16 or wider, within the bound.
A program may use at most 128 MiB of HBM per device.

v0:
```python
import jax
import jax.numpy as jnp
from jax import lax
from jax.sharding import PartitionSpec as P

epsilon = 1e-06


def unit_rows(matrix):
    return matrix * lax.rsqrt(jnp.sum(matrix * matrix, axis=-1, keepdims=True) + epsilon)


def exact_product(form, left, right):
    return jnp.einsum(form, left, right, precision=lax.Precision.HIGHEST)


def visibility(parent):
    sequence_count, proposal_count = parent.shape
    position = jnp.arange(proposal_count, dtype=jnp.int32)
    parent_hot = (parent[:, :, None] == position[None, None, :]).astype(jnp.float32)
    ancestry = []
    for row_index in range(proposal_count):
        ancestor_row = parent_hot[:, row_index, :]
        if row_index > 0:
            earlier = jnp.stack(ancestry, axis=1)
            ancestor_row = ancestor_row + exact_product(
                "bj,bjk->bk", parent_hot[:, row_index, :row_index], earlier
            )
        ancestry.append(ancestor_row)
    ancestor = jnp.stack(ancestry, axis=1)
    chain = (position[:, None] > position[None, :]).astype(jnp.float32)
    upper = jnp.concatenate(
        [
            jnp.broadcast_to(chain, (sequence_count, proposal_count, proposal_count)),
            jnp.zeros((sequence_count, proposal_count, proposal_count), jnp.float32),
        ],
        axis=2,
    )
    lower = jnp.concatenate(
        [jnp.ones((sequence_count, proposal_count, proposal_count), jnp.float32), ancestor], axis=2
    )
    return jnp.concatenate([upper, lower], axis=1)


def split_heads(matrix, sequence_count, proposal_count, number_of_heads):
    return (
        matrix.astype(jnp.float32)
        .reshape(sequence_count, proposal_count, number_of_heads, -1)
        .transpose(0, 2, 1, 3)
    )


def delta_recursion(
    query_projected,
    key_projected,
    value_projected,
    output_gate_logits,
    write_strength_logits,
    decay_logits,
    decay_speed,
    proposal_group,
    head_norm_gain,
    state,
    previous_keys,
    previous_values,
    previous_log_decay,
    previous_strengths,
    accepted,
    parent,
    channel_count_total,
):
    sequence_count, number_of_heads, value_dim, head_dim = state.shape
    proposal_count = parent.shape[1]
    queries = unit_rows(
        split_heads(query_projected, sequence_count, proposal_count, number_of_heads)
    ) * head_dim ** (-0.5)
    new_keys = unit_rows(
        split_heads(key_projected, sequence_count, proposal_count, number_of_heads)
    )
    old_keys = unit_rows(
        split_heads(previous_keys, sequence_count, proposal_count, number_of_heads)
    )
    new_values = split_heads(value_projected, sequence_count, proposal_count, number_of_heads)
    old_values = split_heads(previous_values, sequence_count, proposal_count, number_of_heads)
    zgate = split_heads(output_gate_logits, sequence_count, proposal_count, number_of_heads)
    beta_new = jax.nn.sigmoid(
        write_strength_logits.reshape(sequence_count, proposal_count, number_of_heads)
    ).transpose(0, 2, 1)
    fresh_decay = (
        -decay_speed[None, None, :]
        * jax.nn.softplus(decay_logits.reshape(sequence_count, proposal_count, number_of_heads))
        + proposal_group
    ).transpose(0, 2, 1)
    position = jnp.arange(proposal_count, dtype=jnp.int32)
    live = (position[None, :] < accepted[:, None]).astype(jnp.float32)[:, None, :]
    beta_old = previous_strengths.transpose(0, 2, 1) * live
    decay_old = previous_log_decay.transpose(0, 2, 1) * live
    keys_all = jnp.concatenate([old_keys, new_keys], axis=2)
    values_all = jnp.concatenate([old_values, new_values], axis=2)
    beta_all = jnp.concatenate([beta_old, beta_new], axis=2)
    decay_all = jnp.concatenate([decay_old, fresh_decay], axis=2)
    visible = visibility(parent)
    gamma_sum = decay_all + exact_product("bij,bhj->bhi", visible, decay_all)
    gamma_diff = gamma_sum[:, :, :, None] - gamma_sum[:, :, None, :]
    decay_pair = jnp.exp(jnp.minimum(gamma_diff, 0.0)) * visible[:, None]
    coupling = (
        beta_all[..., None] * exact_product("bhid,bhjd->bhij", keys_all, keys_all) * decay_pair
    )
    right_side = jnp.concatenate(
        [beta_all[..., None] * values_all, (beta_all * jnp.exp(gamma_sum))[..., None] * keys_all],
        axis=-1,
    )
    solved = []
    for row_index in range(2 * proposal_count):
        current = right_side[:, :, row_index]
        if row_index > 0:
            current = current - exact_product(
                "bhj,bhjd->bhd", coupling[:, :, row_index, :row_index], jnp.stack(solved, axis=2)
            )
        solved.append(current)
    solution = jnp.stack(solved, axis=2)
    update = solution[..., :value_dim] - exact_product(
        "bhcd,bhed->bhce", solution[..., value_dim:], state
    )
    identity = jnp.eye(2 * proposal_count, dtype=jnp.float32)
    seen = visible[:, proposal_count:] + identity[proposal_count:][None]
    reach = jnp.exp(jnp.minimum(gamma_diff[:, :, proposal_count:], 0.0)) * seen[:, None]
    query_key = exact_product("bhid,bhjd->bhij", queries, keys_all) * reach
    readout = exact_product(
        "bhid,bhed->bhie", queries * jnp.exp(gamma_sum[:, :, proposal_count:])[..., None], state
    )
    readout = readout + exact_product("bhij,bhje->bhie", query_key, update)
    squares = channel_count_total(jnp.sum(readout * readout, axis=-1))
    readout = readout * lax.rsqrt(squares / head_dim + epsilon)[..., None]
    readout = readout * head_norm_gain.astype(jnp.float32) * jax.nn.silu(zgate)
    blended_rows = readout.transpose(0, 2, 1, 3).reshape(
        sequence_count * proposal_count, number_of_heads * value_dim
    )
    blended_rows = blended_rows.astype(jnp.bfloat16)
    last_gamma = gamma_sum[:, :, proposal_count - 1 : proposal_count]
    key_weighted = old_keys * jnp.exp(last_gamma - gamma_sum[:, :, :proposal_count])[..., None]
    accepted_state = jnp.exp(last_gamma)[..., None] * state + exact_product(
        "bhcd,bhce->bhed", key_weighted, update[:, :, :proposal_count]
    )
    return (blended_rows, accepted_state)


def channel_sum(squares):
    return lax.psum(squares, "tp")


def on_device(
    tokens,
    input_norm_gain,
    query_weight,
    key_weight,
    value_weight,
    output_gate_weight,
    strength_weight,
    decay_weight,
    head_decay_rate,
    proposal_log_decay,
    head_norm_gain,
    output_weight,
    output_norm_gain,
    state,
    previous_keys,
    previous_values,
    previous_log_decay,
    previous_strengths,
    accepted,
    parent,
):
    gathered = lax.all_gather(tokens, ("kv", "tp"), axis=2, tiled=True)
    sequence_count, proposal_count, width = gathered.shape
    row_total = sequence_count * proposal_count
    features = gathered.astype(jnp.float32)
    normed = features * lax.rsqrt(jnp.mean(features * features, axis=-1, keepdims=True) + epsilon)
    normed = (normed * input_norm_gain.astype(jnp.float32)).astype(jnp.bfloat16)
    flat_rows = normed.reshape(row_total, width)
    write_strength_logits = jnp.dot(flat_rows, strength_weight, preferred_element_type=jnp.float32)
    decay_logits = jnp.dot(flat_rows, decay_weight, preferred_element_type=jnp.float32)
    value_projected = jnp.dot(
        flat_rows, value_weight.reshape(width, -1), preferred_element_type=jnp.float32
    ).astype(jnp.bfloat16)
    output_gate_logits = jnp.dot(
        flat_rows, output_gate_weight.reshape(width, -1), preferred_element_type=jnp.float32
    ).astype(jnp.bfloat16)
    query_projected = jnp.dot(flat_rows, query_weight, preferred_element_type=jnp.float32).astype(
        jnp.bfloat16
    )
    key_projected = jnp.dot(flat_rows, key_weight, preferred_element_type=jnp.float32).astype(
        jnp.bfloat16
    )
    blended_rows, accepted_state = delta_recursion(
        query_projected,
        key_projected,
        value_projected,
        output_gate_logits,
        write_strength_logits,
        decay_logits,
        head_decay_rate,
        proposal_log_decay,
        head_norm_gain,
        state,
        previous_keys,
        previous_values,
        previous_log_decay,
        previous_strengths,
        accepted,
        parent,
        channel_sum,
    )
    partial_out = jnp.dot(
        blended_rows, output_weight.reshape(-1, width), preferred_element_type=jnp.float32
    )
    own_cols = output_norm_gain.shape[0]
    totals = lax.psum(partial_out, ("kv", "tp"))
    scaling = lax.rsqrt(jnp.mean(totals * totals, axis=-1, keepdims=True) + epsilon)
    own_index = lax.axis_index("kv") * lax.axis_size("tp") + lax.axis_index("tp")
    share = lax.dynamic_slice_in_dim(totals, own_index * own_cols, own_cols, 1)
    layer_out = (share * scaling * output_norm_gain.astype(jnp.float32)).astype(jnp.bfloat16)
    return (layer_out.reshape(sequence_count, proposal_count, own_cols), accepted_state)


def solution(mesh):
    placed = (
        P(None, None, ("kv", "tp")),
        P(),
        P(None, "kv"),
        P(None, "kv"),
        P(None, "kv", "tp"),
        P(None, "kv", "tp"),
        P(None, "kv"),
        P(None, "kv"),
        P("kv"),
        P(None, None, "kv"),
        P("tp"),
        P("kv", "tp", None),
        P(("kv", "tp")),
        P(None, "kv", "tp", None),
        P(None, None, "kv"),
        P(None, None, "kv", "tp"),
        P(None, None, "kv"),
        P(None, None, "kv"),
        P(),
        P(),
    )
    return jax.shard_map(
        on_device,
        mesh=mesh,
        in_specs=placed,
        out_specs=(P(None, None, ("kv", "tp")), P(None, "kv", "tp", None)),
        check_vma=False,
    )
```

profile of v0, /device:TPU:0, one launch (start us, length us, event | category | flops | bytes accessed | tf_op | source)
XLA Modules:
  0.0 489.5 jit_solution(4462959712660813374)
XLA Ops:
  11.4 2.1 fusion.18
  16.0 1.6 fusion.16
  17.7 58.3 %all-gather.2.cloned.1.call-done = bf16[256,4,2048]{0,2,1:T(8,128)(2,1)} async-done(((bf16[256,4,64]{0,2,1:T(8,128)(2,1)}), bf16[256,4,2048]{0,2,1:T(8,128)(2,1)}) %all-gather.2.cloned.1.call-update) | async-done | bytes 4194320 | tf_op jit(solution)/shard_map/all_gather | solution.py:174
  76.1 3.2 fusion
  79.5 2.7 fusion.2
  82.2 7.9 %copy.594 = bf16[256,4,2048]{2,1,0:T(4,128)(2,1)} copy(bf16[256,4,2048]{0,2,1:T(8,128)(2,1)} %fusion.2) | data formatting | bytes 8388608 | tf_op jit(solution)/shard_map/convert_element_type | solution.py:179
  90.2 3.0 fusion.61
  94.6 2.5 fusion.94
  98.4 6.9 %reshape.134 = bf16[1024,2048]{1,0:T(8,128)(2,1)} reshape(bf16[256,4,2048]{2,1,0:T(4,128)(2,1)} %copy.594) | data formatting | bytes 8388608 | tf_op jit(solution)/shard_map/reshape | solution.py:180
  105.2 3.4 fusion.9
  111.1 1.7 bitcast_multiply_fusion
  112.8 1.7 broadcast_subtract_fusion
  115.3 5.3 %multiply_multiply_fusion = f32[256,2,8,8]{3,2,1,0:T(8,128)S(1)} fusion(f32[256,2,4,128]{3,2,1,0:T(4,128)S(1)} %bitcast_multiply_fusion, f32[256,2,4,128]{3,2,1,0:T(4,128)S(1)} %fusion.16, f32[256,8,8]{2,1,0:T(8,128)S(1)} %copy-done.22, f32[256,2,8]{2,1,0:T(2,128)} %copy.621, f32[256,2,8]{2,1,0:T(2,128)S(1)} %copy.615), kind=kOutput, calls=%fused_computation.26 | convolution fusion | flops 51019776 | bytes 2326528 | tf_op jit(solution)/shard_map/bhid,bhjd->bhij/dot_general | solution.py:14
  124.4 1.4 fusion.11
  126.6 1.4 copy.663
  128.1 3.4 fusion.10
  133.5 15.6 %fusion.22 = f32[256,2,4,32]{3,2,1,0:T(4,128)S(1)} fusion(f32[256,2,32,128]{3,2,1,0:T(8,128)} %param.33, f32[256,4,2,128]{3,2,1,0:T(2,128)S(1)} %reshape.152, f32[256,2,4]{2,1,0:T(2,128)S(1)} %copy.609, f32[256,2,4]{2,1,0:T(2,128)S(1)} %copy.597), kind=kOutput, calls=%fused_computation.58 | convolution fusion | flops 101187584 | bytes 9715712 | tf_op jit(solution)/shard_map/bhid,bhed->bhie/dot_general | solution.py:14
  150.5 1.9 fusion.8
  155.5 1.7 convert_multiply_fusion.2
  157.2 10.5 %pad_maximum_fusion.7 = (f32[256,2,1,160]{3,2,1,0:T(1,128)}, f32[256,2,1,160]{3,2,1,0:T(1,128)S(1)}, f32[256,2,1,160]{3,2,1,0:T(1,128)S(1)}, f32[256,2,1,160]{3,...) fusion(f32[256,2,8,128]{3,2,1,0:T(8,128)S(1)} %fusion.8, ...), kind=kLoop, calls=%fused_computation.72 | loop fusion | flops 655360 | bytes 5242880 | tf_op jit(solution)/shard_map/concatenate | solution.py:109
  170.8 7.6 %fusion.24 = f32[256,2,1,160]{3,2,1,0:T(1,128)} fusion(f32[256,2,1,160]{3,2,1,0:T(1,128)S(1)} %copy.650, f32[256,2,1,160]{3,2,1,0:T(1,128)S(1)} %get-tuple-element.41, f32[256,2,8,8]{3,2,1,0:T(8,128)} %copy-done.6), kind=kOutput, calls=%fused_computation.60 | convolution fusion | flops 2129920 | bytes 1245184 | tf_op jit(solution)/shard_map/bhj,bhjd->bhd/dot_general | solution.py:14
  182.9 2.0 copy.633
  184.9 1.9 constant_dynamic-update-slice_fusion.7
  186.8 2.1 copy.652
  188.9 8.4 %fusion.5 = f32[256,2,1,160]{3,2,1,0:T(1,128)} fusion(f32[256,2,1,160]{3,2,1,0:T(1,128)} %copy.652, f32[256,2,1,160]{3,2,1,0:T(1,128)} %copy.651, f32[256,2,1,160]{3,2,1,0:T(1,128)} %copy-done.8, f32[256,2,1,160]{3,2,1,0:T(1,128)S(1)} %get-tuple-element.41, f32[256,2,8,8]{3,2,1,0:T(8,128)S(1)} %copy-done.7), kind=kOutput, calls=%fused_computation.28 | convolution fusion | flops 4915200 | bytes 2097152 | tf_op jit(solution)/shard_map/bhj,bhjd->bhd/dot_general | solution.py:14
  197.3 1.8 copy.686
  199.1 1.8 copy.635
  201.0 1.9 constant_dynamic-update-slice_fusion.6
  202.9 1.9 copy.653
  206.4 1.7 constant_dynamic-update-slice_fusion.1
  210.3 1.6 multiply_reduce_fusion.2
  212.9 1.9 copy.654
  216.3 1.8 multiply_reduce_fusion.1
  218.9 1.9 copy.655
  220.7 11.4 %stack.101 = f32[256,2,7,160]{3,2,1,0:T(8,128)} concatenate(f32[256,2,1,160]{3,2,1,0:T(1,128)S(1)} %get-tuple-element.41, f32[256,2,1,160]{3,2,1,0:T(1,128)S(1)} %copy-done.9, f32[256,2,1,160]{3,2,1,0:T(1,128)} %copy.651, f32[256,2,1,160]{3,2,1,0:T(1,128)} %copy.652, f32[256,2,1,160]{3,2,1,0:T(1,128)} %copy.653, f32[256,2,1,160]{3,2,1,0:T(1,128)} %copy.654, f32[256,2,1,160]{3,2,1,0:T(1,128)} %copy.655), dimensions={2} | concatenate | bytes 4587520 | tf_op jit(solution)/shard_map/stack | solution.py:118
  232.2 7.2 %fusion.48 = f32[256,2,1,160]{3,2,1,0:T(1,128)} fusion(f32[256,2,7,160]{3,2,1,0:T(8,128)} %stack.101, f32[256,2,8,8]{3,2,1,0:T(8,128)S(1)} %copy-done.7), kind=kOutput, calls=%fused_computation.96 | convolution fusion | flops 6881280 | bytes 2883584 | tf_op jit(solution)/shard_map/bhj,bhjd->bhd/dot_general | solution.py:14
  240.7 1.9 copy.643
  242.5 1.7 fusion.40
  244.3 1.9 copy.656
  246.2 11.2 %stack.103 = f32[256,2,8,160]{3,2,1,0:T(8,128)} concatenate(f32[256,2,1,160]{3,2,1,0:T(1,128)S(1)} %get-tuple-element.41, f32[256,2,1,160]{3,2,1,0:T(1,128)S(1)} %copy-done.9, f32[256,2,1,160]{3,2,1,0:T(1,128)S(1)} %copy-done.10, f32[256,2,1,160]{3,2,1,0:T(1,128)S(1)} %copy-done.11, f32[256,2,1,160]{3,2,1,0:T(1,128)S(1)} %copy-done.12, f32[256,2,1,160]{3,2,1,0:T(1,128)S(1)} %copy-done.13, ...), dimensions={2} | concatenate | bytes 5242880 | tf_op jit(solution)/shard_map/stack | solution.py:121
  257.4 16.8 %slice_subtract_fusion = f32[256,2,8,32]{3,2,1,0:T(8,128)S(1)} fusion(f32[256,2,8,160]{3,2,1,0:T(8,128)} %stack.103, f32[256,2,32,128]{3,2,1,0:T(8,128)} %param.33), kind=kOutput, calls=%fused_computation.23 | convolution fusion | flops 201457664 | bytes 11534336 | tf_op jit(solution)/shard_map/bhcd,bhed->bhce/dot_general | solution.py:14
  274.3 4.2 convolution_multiply_fusion
  278.6 3.4 fusion.95
  284.3 6.4 %psum.14 = f32[256,2,4]{0,2,1:T(4,128)S(1)} all-reduce(f32[256,2,4]{0,2,1:T(4,128)S(1)} %copy.659), channel_id=1, replica_groups=mesh['kv'=8,'tp'=4] {'tp'}, use_global_device_ids=true, to_apply=%region_5.6 | all-reduce | flops 2048 | bytes 16384 | tf_op jit(solution)/shard_map/psum | solution.py:149
  292.8 4.5 fusion.96
  298.4 18.9 %multiply_add_fusion = f32[256,2,32,128]{3,2,1,0:T(8,128)} fusion(f32[256,2,32,128]{3,2,1,0:T(8,128)} %param.33, f32[256,2]{1,0:T(8,128)S(1)} %bitcast.222, f32[256,2,8,32]{3,2,1,0:T(8,128)S(1)} %slice_subtract_fusion, f32[256,2,4]{2,1,0:T(2,128)S(1)} %copy.666, bf16[256,4,256]{2,1,0:T(4,128)(2,1)S(1)} %copy-done.26, f32[256,2,4]{2,1,0:T(2,128)S(1)} %copy-done.32), kind=kOutput, calls=%fused_computation.19 | convolution fusion | flops 105644032 | bytes 19005440 | tf_op jit(solution)/shard_map/bhcd,bhce->bhed/dot_general | solution.py:14
  317.2 158.6 %all-reduce.4.cloned.1.call-done = f32[1024,2048]{1,0:T(8,128)} async-done(((f32[1024,2048]{1,0:T(8,128)}), f32[1024,2048]{1,0:T(8,128)}) %all-reduce.4.cloned.1.call-update) | async-done | bytes 8388624 | tf_op jit(solution)/shard_map/psum | solution.py:218
  475.8 4.1 multiply_reduce_fusion
  (202 shorter events, 47.0 us)
Async XLA Ops:
  7.2 98.1 %copy-start = (bf16[2048,256]{1,0:T(8,128)(2,1)S(1)}, bf16[2048,256]{1,0:T(8,128)(2,1)}, u32[]{:S(2)}) copy-start(bf16[2048,256]{1,0:T(8,128)(2,1)} %param.23) | copy-start | bytes 3145732
  7.2 7.7 %copy-start.41 = (bf16[256,4,2,32]{0,3,2,1:T(8,128)(2,1)S(1)}, bf16[256,4,2,32]{0,3,2,1:T(8,128)(2,1)}, u32[]{:S(2)}) copy-start(bf16[256,4,2,32]{0,3,2,1:T(8,128)(2,1)} %param.35) | copy-start | bytes 393220
  7.2 8.8 %copy-start.47 = (s32[256]{0:T(256)S(1)}, s32[256]{0:T(256)}, u32[]{:S(2)}) copy-start(s32[256]{0:T(256)} %param.38) | copy-start | bytes 3076
  7.2 8.8 %copy-start.44 = (f32[256,4,2]{0,2,1:T(2,128)S(1)}, f32[256,4,2]{0,2,1:T(2,128)}, u32[]{:S(2)}) copy-start(f32[256,4,2]{0,2,1:T(2,128)} %param.36) | copy-start | bytes 24580
  7.2 8.8 %copy-start.45 = (f32[256,4,2]{0,2,1:T(2,128)S(1)}, f32[256,4,2]{0,2,1:T(2,128)}, u32[]{:S(2)}) copy-start(f32[256,4,2]{0,2,1:T(2,128)} %param.37) | copy-start | bytes 24580
  7.2 68.8 %all-gather.2.cloned.1.call-start = ((), (), s32[]{:S(2)}) async-start(), calls=%async_computation | async-start | bytes 4325376 | tf_op jit(solution)/shard_map/all_gather | solution.py:174
  8.0 467.8 %all-reduce.4.cloned.1.call-start = ((), (), s32[]{:S(2)}) async-start(), calls=%async_computation.1 | async-start | bytes 16777216 | tf_op jit(solution)/shard_map/psum | solution.py:218
  11.4 83.1 %copy-start.21 = (f32[256,8,8]{2,1,0:T(8,128)}, f32[256,8,8]{2,1,0:T(8,128)S(1)}, u32[]{:S(2)}) copy-start(f32[256,8,8]{2,1,0:T(8,128)S(1)} %copy.607) | copy-start | bytes 196612
  13.9 65.3 %copy-start.31 = (f32[256,2,4]{2,1,0:T(2,128)}, f32[256,2,4]{2,1,0:T(2,128)S(1)}, u32[]{:S(2)}) copy-start(f32[256,2,4]{2,1,0:T(2,128)S(1)} %copy.611) | copy-start | bytes 24580
  17.7 97.6 %copy-start.14 = (f32[256,2,4,128]{3,2,1,0:T(4,128)}, f32[256,2,4,128]{3,2,1,0:T(4,128)S(1)}, u32[]{:S(2)}) copy-start(f32[256,2,4,128]{3,2,1,0:T(4,128)S(1)} %fusion.16) | copy-start | bytes 3145732
  76.1 3.4 copy-start.5
  82.2 7.9 %copy-start.42 = (bf16[2048,2]{0,1:T(2,128)(2,1)S(1)}, bf16[2048,2]{0,1:T(2,128)(2,1)}, u32[]{:S(2)}) copy-start(bf16[2048,2]{0,1:T(2,128)(2,1)} %param.27) | copy-start | bytes 24580
  90.2 3.4 copy-start.2
  90.2 3.5 copy-start.43
  112.8 7.9 %copy-start.17 = (f32[256,2,4,128]{3,2,1,0:T(4,128)}, f32[256,2,4,128]{3,2,1,0:T(4,128)S(1)}, u32[]{:S(2)}) copy-start(f32[256,2,4,128]{3,2,1,0:T(4,128)S(1)} %bitcast_multiply_fusion) | copy-start | bytes 3145732
  112.8 2.5 copy-start.22
  115.3 9.1 %copy-start.3 = (bf16[1024,2048]{1,0:T(8,128)(2,1)S(1)}, bf16[1024,2048]{1,0:T(8,128)(2,1)}, u32[]{:S(2)}) copy-start(bf16[1024,2048]{1,0:T(8,128)(2,1)} %reshape.134) | copy-start | bytes 12582916
  120.7 2.8 copy-start.6
  120.7 3.7 copy-start.36
  125.8 2.3 copy-start.48
  132.1 1.4 copy-start.19
  133.5 15.6 %copy-start.39 = (f32[256,2,4]{2,1,0:T(2,128)}, f32[256,2,4]{2,1,0:T(2,128)S(1)}, u32[]{:S(2)}) copy-start(f32[256,2,4]{2,1,0:T(2,128)S(1)} %copy.597) | copy-start | bytes 24580
  149.1 1.4 copy-start.15
  150.5 2.5 copy-start.4
  150.5 2.5 copy-start.37
  157.2 11.8 %copy-start.34 = (f32[256,2,1,1]{3,2,1,0:T(1,128)S(1)}, f32[256,2,1,1]{3,2,1,0:T(1,128)}, u32[]{:S(2)}) copy-start(f32[256,2,1,1]{3,2,1,0:T(1,128)} %slice.141) | copy-start | bytes 6148
  170.8 7.6 %copy-start.8 = (f32[256,2,1,160]{3,2,1,0:T(1,128)}, f32[256,2,1,160]{3,2,1,0:T(1,128)S(1)}, u32[]{:S(2)}) copy-start(f32[256,2,1,160]{3,2,1,0:T(1,128)S(1)} %copy.650) | copy-start | bytes 983044
  170.8 8.9 %copy-start.29 = (f32[256,2,1,160]{3,2,1,0:T(1,128)S(1)}, f32[256,2,1,160]{3,2,1,0:T(1,128)}, u32[]{:S(2)}) copy-start(f32[256,2,1,160]{3,2,1,0:T(1,128)} %get-tuple-element.43) | copy-start | bytes 983044
  178.4 3.5 copy-start.33
  182.9 6.0 %copy-start.7 = (f32[256,2,8,8]{3,2,1,0:T(8,128)S(1)}, f32[256,2,8,8]{3,2,1,0:T(8,128)}, u32[]{:S(2)}) copy-start(f32[256,2,8,8]{3,2,1,0:T(8,128)} %copy-done.6) | copy-start | bytes 393220
  204.8 3.2 copy-start.23
  205.6 4.3 copy-start.28
  210.3 5.5 %copy-start.27 = (f32[256,2,1,160]{3,2,1,0:T(1,128)S(1)}, f32[256,2,1,160]{3,2,1,0:T(1,128)}, u32[]{:S(2)}) copy-start(f32[256,2,1,160]{3,2,1,0:T(1,128)} %get-tuple-element.47) | copy-start | bytes 983044
  216.3 4.5 copy-start.9
  239.3 6.8 %copy-start.10 = (f32[256,2,1,160]{3,2,1,0:T(1,128)S(1)}, f32[256,2,1,160]{3,2,1,0:T(1,128)}, u32[]{:S(2)}) copy-start(f32[256,2,1,160]{3,2,1,0:T(1,128)} %copy.651) | copy-start | bytes 983044
  239.3 6.9 %copy-start.11 = (f32[256,2,1,160]{3,2,1,0:T(1,128)S(1)}, f32[256,2,1,160]{3,2,1,0:T(1,128)}, u32[]{:S(2)}) copy-start(f32[256,2,1,160]{3,2,1,0:T(1,128)} %copy.652) | copy-start | bytes 983044
  239.3 6.9 %copy-start.12 = (f32[256,2,1,160]{3,2,1,0:T(1,128)S(1)}, f32[256,2,1,160]{3,2,1,0:T(1,128)}, u32[]{:S(2)}) copy-start(f32[256,2,1,160]{3,2,1,0:T(1,128)} %copy.653) | copy-start | bytes 983044
  239.3 6.9 %copy-start.13 = (f32[256,2,1,160]{3,2,1,0:T(1,128)S(1)}, f32[256,2,1,160]{3,2,1,0:T(1,128)}, u32[]{:S(2)}) copy-start(f32[256,2,1,160]{3,2,1,0:T(1,128)} %copy.654) | copy-start | bytes 983044
  257.3 16.9 %copy-start.16 = (f32[256,2,4,128]{3,2,1,0:T(4,128)S(1)}, f32[256,2,4,128]{3,2,1,0:T(4,128)}, u32[]{:S(2)}) copy-start(f32[256,2,4,128]{3,2,1,0:T(4,128)} %copy-done.14) | copy-start | bytes 3145732
  257.4 16.9 %copy-start.18 = (f32[256,2,4,128]{3,2,1,0:T(4,128)S(1)}, f32[256,2,4,128]{3,2,1,0:T(4,128)}, u32[]{:S(2)}) copy-start(f32[256,2,4,128]{3,2,1,0:T(4,128)} %copy-done.17) | copy-start | bytes 3145732
  257.4 16.9 %copy-start.20 = (f32[256,4,2,128]{3,2,1,0:T(2,128)S(1)}, f32[256,4,2,128]{3,2,1,0:T(2,128)}, u32[]{:S(2)}) copy-start(f32[256,4,2,128]{3,2,1,0:T(2,128)} %copy-done.19) | copy-start | bytes 3145732
  257.4 16.9 %copy-start.25 = (f32[256,2,8,8]{3,2,1,0:T(8,128)S(1)}, f32[256,2,8,8]{3,2,1,0:T(8,128)}, u32[]{:S(2)}) copy-start(f32[256,2,8,8]{3,2,1,0:T(8,128)} %broadcast_subtract_fusion) | copy-start | bytes 393220
  257.4 16.9 %copy-start.35 = (f32[256,4,8]{2,1,0:T(4,128)S(1)}, f32[256,4,8]{2,1,0:T(4,128)}, u32[]{:S(2)}) copy-start(f32[256,4,8]{2,1,0:T(4,128)} %copy.617) | copy-start | bytes 98308
  257.4 16.9 %copy-start.40 = (f32[256,2,4]{2,1,0:T(2,128)S(1)}, f32[256,2,4]{2,1,0:T(2,128)}, u32[]{:S(2)}) copy-start(f32[256,2,4]{2,1,0:T(2,128)} %copy-done.39) | copy-start | bytes 24580
  278.6 4.6 copy-start.24
  283.2 9.6 %copy-start.38 = (bf16[2,32,2048]{2,1,0:T(8,128)(2,1)S(1)}, bf16[2,32,2048]{2,1,0:T(8,128)(2,1)}, u32[]{:S(2)}) copy-start(bf16[2,32,2048]{2,1,0:T(8,128)(2,1)} %param.31) | copy-start | bytes 786436
  297.2 1.1 copy-start.32
  475.8 6.3 %copy-start.1 = (bf16[2048,256]{1,0:T(8,128)(2,1)S(1)}, bf16[2048,256]{1,0:T(8,128)(2,1)}, u32[]{:S(2)}) copy-start(bf16[2048,256]{1,0:T(8,128)(2,1)} %param.23) | copy-start | bytes 3145732
  (4 other events, 3.5 us)
Sparse Core Ops, SparseCore 0:
  10.9 65.0 all-gather.1
  297.4 178.3 all-reduce.3
where the time goes:
time: 496 us; the launch traced here: 489 us
  waiting for transfers between devices  218 us (44%)
  matrix products  108 us (22%)
  local copies, waits for them, and re-layouts  89.5 us (18%)
  other arithmetic  52.6 us (11%)
  between operations  15.5 us (3%)
  blocking collectives  6.36 us (1%)
    psum x1, waiting for transfers between devices, on_device(): totals = lax.psum(partial_out, ('kv', 'tp'))  159 us
    dot_general x10, matrix products, exact_product(): return jnp.einsum(form, left, right, precision=lax.Precision.HIGHEST)  90 us
    all_gather x1, waiting for transfers between devices, on_device(): gathered = lax.all_gather(tokens, ('kv', 'tp'), axis=2, tiled=True)  58.3 us
    another operation x8, local copies, waits for them, and re-layouts, delta_recursion(): solution = jnp.stack(solved, axis=2)  22.3 us
    another operation x2, local copies, waits for them, and re-layouts, delta_recursion(): jnp.stack(solved, axis=2)  12.1 us
    unnamed x110, local copies, waits for them, and re-layouts  11 us
    concatenate x1, other arithmetic, delta_recursion(): jnp.concatenate([beta_all[..., None] * values_all, (beta_all * jnp.exp(ga...  10.5 us
  transfers between devices with their start and end apart: 2, of which 2 were waited for; matrix products, arithmetic and copies ran while one was open for 6% of the time, Pallas kernels for 0%

commit v1 on v0

--- a/solution.py
+++ b/solution.py
@@ -215,7 +215,8 @@
         blended_rows, output_weight.reshape(-1, width), preferred_element_type=jnp.float32
     )
     own_cols = output_norm_gain.shape[0]
-    totals = lax.psum(partial_out, ("kv", "tp"))
+    _carry_sheet = lambda chunk, bus_axis, net_axis: lax.psum(lax.psum(chunk, bus_axis), net_axis)
+    totals = _carry_sheet(partial_out, "kv", "tp")
     scaling = lax.rsqrt(jnp.mean(totals * totals, axis=-1, keepdims=True) + epsilon)
     own_index = lax.axis_index("kv") * lax.axis_size("tp") + lax.axis_index("tp")
     share = lax.dynamic_slice_in_dim(totals, own_index * own_cols, own_cols, 1)

time: 496 us -> 741 us (1.49)
  waiting for transfers between devices: 218 us -> 463 us
    psum x1 -> x2, waiting for transfers between devices: 159 us -> 404 us  [the longest x1 269 us: on_device(): lax.psum(chunk, bus_axis)]
  transfers between devices with their start and end apart: 2 -> 3, of which waited for: 2 -> 3; matrix products, arithmetic and copies ran while one was open for 6% -> 4% of each run, Pallas kernels for 0% -> 0%
where the time goes in v1:
time: 741 us; the launch traced here: 734 us
  waiting for transfers between devices  463 us (62%)
  matrix products  108 us (15%)
  local copies, waits for them, and re-layouts  89.2 us (12%)
  other arithmetic  52.6 us (7%)
  between operations  15.2 us (2%)
    psum x1, waiting for transfers between devices, on_device(): lax.psum(chunk, bus_axis)  269 us
    psum x1, waiting for transfers between devices, on_device(): lax.psum(lax.psum(chunk, bus_axis), net_axis)  134 us
    dot_general x10, matrix products, exact_product(): return jnp.einsum(form, left, right, precision=lax.Precision.HIGHEST)  90.3 us
    all_gather x1, waiting for transfers between devices, on_device(): gathered = lax.all_gather(tokens, ('kv', 'tp'), axis=2, tiled=True)  58.3 us
    another operation x8, local copies, waits for them, and re-layouts, delta_recursion(): solution = jnp.stack(solved, axis=2)  22.3 us
  transfers between devices with their start and end apart: 3, of which 3 were waited for; matrix products, arithmetic and copies ran while one was open for 4% of the time, Pallas kernels for 0%

profile of v1, /device:TPU:0, one launch (start us, length us, event | category | flops | bytes accessed | tf_op | source)
XLA Modules:
  0.0 734.5 jit_solution(16359781349255441863)
XLA Ops:
  11.4 2.1 fusion.18
  16.0 1.6 fusion.16
  17.7 58.3 %all-gather.2.cloned.1.call-done = bf16[256,4,2048]{0,2,1:T(8,128)(2,1)} async-done(((bf16[256,4,64]{0,2,1:T(8,128)(2,1)}), bf16[256,4,2048]{0,2,1:T(8,128)(2,1)}) %all-gather.2.cloned.1.call-update) | async-done | bytes 4194320 | tf_op jit(solution)/shard_map/all_gather | solution.py:174
  76.1 3.2 fusion
  79.5 2.7 fusion.2
  82.2 7.9 %copy.594 = bf16[256,4,2048]{2,1,0:T(4,128)(2,1)} copy(bf16[256,4,2048]{0,2,1:T(8,128)(2,1)} %fusion.2) | data formatting | bytes 8388608 | tf_op jit(solution)/shard_map/convert_element_type | solution.py:179
  90.2 3.0 fusion.61
  94.6 2.5 fusion.94
  98.4 6.9 reshape.134
  105.2 3.4 fusion.9
  111.1 1.7 bitcast_multiply_fusion
  112.8 1.7 broadcast_subtract_fusion
  115.3 5.3 multiply_multiply_fusion
  126.6 1.4 copy.663
  128.1 3.4 fusion.10
  133.5 15.6 %fusion.22 = f32[256,2,4,32]{3,2,1,0:T(4,128)S(1)} fusion(f32[256,2,32,128]{3,2,1,0:T(8,128)} %param.33, f32[256,4,2,128]{3,2,1,0:T(2,128)S(1)} %reshape.152, f32[256,2,4]{2,1,0:T(2,128)S(1)} %copy.609, f32[256,2,4]{2,1,0:T(2,128)S(1)} %copy.597), kind=kOutput, calls=%fused_computation.58 | convolution fusion | flops 101187584 | bytes 9715712 | tf_op jit(solution)/shard_map/bhid,bhed->bhie/dot_general | solution.py:14
  150.5 1.9 fusion.8
  155.5 1.7 convert_multiply_fusion.2
  157.2 10.5 %pad_maximum_fusion.7 = (f32[256,2,1,160]{3,2,1,0:T(1,128)}, f32[256,2,1,160]{3,2,1,0:T(1,128)S(1)}, f32[256,2,1,160]{3,2,1,0:T(1,128)S(1)}, f32[256,2,1,160]{3,...) fusion(f32[256,2,8,128]{3,2,1,0:T(8,128)S(1)} %fusion.8, ...), kind=kLoop, calls=%fused_computation.72 | loop fusion | flops 655360 | bytes 5242880 | tf_op jit(solution)/shard_map/concatenate | solution.py:109
  170.8 7.6 %fusion.24 = f32[256,2,1,160]{3,2,1,0:T(1,128)} fusion(f32[256,2,1,160]{3,2,1,0:T(1,128)S(1)} %copy.650, f32[256,2,1,160]{3,2,1,0:T(1,128)S(1)} %get-tuple-element.41, f32[256,2,8,8]{3,2,1,0:T(8,128)} %copy-done.6), kind=kOutput, calls=%fused_computation.60 | convolution fusion | flops 2129920 | bytes 1245184 | tf_op jit(solution)/shard_map/bhj,bhjd->bhd/dot_general | solution.py:14
  182.9 2.0 copy.633
  184.9 1.9 constant_dynamic-update-slice_fusion.7
  186.8 2.1 copy.652
  188.9 8.4 %fusion.5 = f32[256,2,1,160]{3,2,1,0:T(1,128)} fusion(f32[256,2,1,160]{3,2,1,0:T(1,128)} %copy.652, f32[256,2,1,160]{3,2,1,0:T(1,128)} %copy.651, f32[256,2,1,160]{3,2,1,0:T(1,128)} %copy-done.8, f32[256,2,1,160]{3,2,1,0:T(1,128)S(1)} %get-tuple-element.41, f32[256,2,8,8]{3,2,1,0:T(8,128)S(1)} %copy-done.7), kind=kOutput, calls=%fused_computation.28 | convolution fusion | flops 4915200 | bytes 2097152 | tf_op jit(solution)/shard_map/bhj,bhjd->bhd/dot_general | solution.py:14
  197.3 1.8 copy.686
  199.1 1.8 copy.635
  201.0 1.9 constant_dynamic-update-slice_fusion.6
  202.9 1.9 copy.653
  206.4 1.7 constant_dynamic-update-slice_fusion.1
  210.3 1.6 multiply_reduce_fusion.2
  212.9 1.9 copy.654
  216.3 1.8 multiply_reduce_fusion.1
  218.9 1.9 copy.655
  220.7 11.4 %stack.101 = f32[256,2,7,160]{3,2,1,0:T(8,128)} concatenate(f32[256,2,1,160]{3,2,1,0:T(1,128)S(1)} %get-tuple-element.41, f32[256,2,1,160]{3,2,1,0:T(1,128)S(1)} %copy-done.9, f32[256,2,1,160]{3,2,1,0:T(1,128)} %copy.651, f32[256,2,1,160]{3,2,1,0:T(1,128)} %copy.652, f32[256,2,1,160]{3,2,1,0:T(1,128)} %copy.653, f32[256,2,1,160]{3,2,1,0:T(1,128)} %copy.654, f32[256,2,1,160]{3,2,1,0:T(1,128)} %copy.655), dimensions={2} | concatenate | bytes 4587520 | tf_op jit(solution)/shard_map/stack | solution.py:118
  232.2 7.2 fusion.48
  240.7 1.9 copy.643
  242.5 1.7 fusion.40
  244.3 1.9 copy.656
  246.2 11.2 %stack.103 = f32[256,2,8,160]{3,2,1,0:T(8,128)} concatenate(f32[256,2,1,160]{3,2,1,0:T(1,128)S(1)} %get-tuple-element.41, f32[256,2,1,160]{3,2,1,0:T(1,128)S(1)} %copy-done.9, f32[256,2,1,160]{3,2,1,0:T(1,128)S(1)} %copy-done.10, f32[256,2,1,160]{3,2,1,0:T(1,128)S(1)} %copy-done.11, f32[256,2,1,160]{3,2,1,0:T(1,128)S(1)} %copy-done.12, f32[256,2,1,160]{3,2,1,0:T(1,128)S(1)} %copy-done.13, ...), dimensions={2} | concatenate | bytes 5242880 | tf_op jit(solution)/shard_map/stack | solution.py:121
  257.4 16.8 %slice_subtract_fusion = f32[256,2,8,32]{3,2,1,0:T(8,128)S(1)} fusion(f32[256,2,8,160]{3,2,1,0:T(8,128)} %stack.103, f32[256,2,32,128]{3,2,1,0:T(8,128)} %param.33), kind=kOutput, calls=%fused_computation.23 | convolution fusion | flops 201457664 | bytes 11534336 | tf_op jit(solution)/shard_map/bhcd,bhed->bhce/dot_general | solution.py:14
  274.3 4.2 convolution_multiply_fusion
  278.6 3.4 fusion.95
  284.3 6.4 psum.21
  292.5 4.6 fusion.96
  297.2 269.5 %all-reduce.5.cloned.1.call-done = f32[1024,2048]{1,0:T(8,128)} async-done(((f32[1024,2048]{1,0:T(8,128)}), f32[1024,2048]{1,0:T(8,128)}) %all-reduce.5.cloned.1.call-update) | async-done | bytes 8388624 | tf_op jit(solution)/shard_map/psum | solution.py:218
  567.8 19.1 %multiply_add_fusion = f32[256,2,32,128]{3,2,1,0:T(8,128)} fusion(f32[256,2,32,128]{3,2,1,0:T(8,128)} %param.33, f32[256,2]{1,0:T(8,128)S(1)} %bitcast.222, f32[256,2,8,32]{3,2,1,0:T(8,128)S(1)} %slice_subtract_fusion, f32[256,2,4]{2,1,0:T(2,128)S(1)} %copy.666, bf16[256,4,256]{2,1,0:T(4,128)(2,1)S(1)} %copy-done.26, f32[256,2,4]{2,1,0:T(2,128)S(1)} %copy-done.32), kind=kOutput, calls=%fused_computation.19 | convolution fusion | flops 105644032 | bytes 19005440 | tf_op jit(solution)/shard_map/bhcd,bhce->bhed/dot_general | solution.py:14
  586.9 134.2 %all-reduce.7.cloned.1.call-done = f32[1024,2048]{1,0:T(8,128)} async-done(((f32[1024,2048]{1,0:T(8,128)}), f32[1024,2048]{1,0:T(8,128)}) %all-reduce.7.cloned.1.call-update) | async-done | bytes 8388624 | tf_op jit(solution)/shard_map/psum | solution.py:218
  721.1 4.1 multiply_reduce_fusion
  (205 shorter events, 48.2 us)
Async XLA Ops:
  7.2 98.1 %copy-start = (bf16[2048,256]{1,0:T(8,128)(2,1)S(1)}, bf16[2048,256]{1,0:T(8,128)(2,1)}, u32[]{:S(2)}) copy-start(bf16[2048,256]{1,0:T(8,128)(2,1)} %param.23) | copy-start | bytes 3145732
  7.2 7.7 %copy-start.41 = (bf16[256,4,2,32]{0,3,2,1:T(8,128)(2,1)S(1)}, bf16[256,4,2,32]{0,3,2,1:T(8,128)(2,1)}, u32[]{:S(2)}) copy-start(bf16[256,4,2,32]{0,3,2,1:T(8,128)(2,1)} %param.35) | copy-start | bytes 393220
  7.2 8.8 %copy-start.47 = (s32[256]{0:T(256)S(1)}, s32[256]{0:T(256)}, u32[]{:S(2)}) copy-start(s32[256]{0:T(256)} %param.38) | copy-start | bytes 3076
  7.2 8.8 %copy-start.44 = (f32[256,4,2]{0,2,1:T(2,128)S(1)}, f32[256,4,2]{0,2,1:T(2,128)}, u32[]{:S(2)}) copy-start(f32[256,4,2]{0,2,1:T(2,128)} %param.36) | copy-start | bytes 24580
  7.2 8.8 %copy-start.45 = (f32[256,4,2]{0,2,1:T(2,128)S(1)}, f32[256,4,2]{0,2,1:T(2,128)}, u32[]{:S(2)}) copy-start(f32[256,4,2]{0,2,1:T(2,128)} %param.37) | copy-start | bytes 24580
  7.2 68.8 %all-gather.2.cloned.1.call-start = ((), (), s32[]{:S(2)}) async-start(), calls=%async_computation | async-start | bytes 4325376 | tf_op jit(solution)/shard_map/all_gather | solution.py:174
  8.0 558.7 %all-reduce.5.cloned.1.call-start = ((), (), s32[]{:S(2)}) async-start(), calls=%async_computation.1 | async-start | bytes 16777216 | tf_op jit(solution)/shard_map/psum | solution.py:218
  11.4 83.1 %copy-start.21 = (f32[256,8,8]{2,1,0:T(8,128)}, f32[256,8,8]{2,1,0:T(8,128)S(1)}, u32[]{:S(2)}) copy-start(f32[256,8,8]{2,1,0:T(8,128)S(1)} %copy.607) | copy-start | bytes 196612
  13.9 65.3 %copy-start.31 = (f32[256,2,4]{2,1,0:T(2,128)}, f32[256,2,4]{2,1,0:T(2,128)S(1)}, u32[]{:S(2)}) copy-start(f32[256,2,4]{2,1,0:T(2,128)S(1)} %copy.611) | copy-start | bytes 24580
  17.7 97.6 %copy-start.14 = (f32[256,2,4,128]{3,2,1,0:T(4,128)}, f32[256,2,4,128]{3,2,1,0:T(4,128)S(1)}, u32[]{:S(2)}) copy-start(f32[256,2,4,128]{3,2,1,0:T(4,128)S(1)} %fusion.16) | copy-start | bytes 3145732
  76.1 3.4 copy-start.5
  82.2 7.9 %copy-start.42 = (bf16[2048,2]{0,1:T(2,128)(2,1)S(1)}, bf16[2048,2]{0,1:T(2,128)(2,1)}, u32[]{:S(2)}) copy-start(bf16[2048,2]{0,1:T(2,128)(2,1)} %param.27) | copy-start | bytes 24580
  90.2 3.4 copy-start.2
  90.2 3.5 copy-start.43
  112.8 7.9 %copy-start.17 = (f32[256,2,4,128]{3,2,1,0:T(4,128)}, f32[256,2,4,128]{3,2,1,0:T(4,128)S(1)}, u32[]{:S(2)}) copy-start(f32[256,2,4,128]{3,2,1,0:T(4,128)S(1)} %bitcast_multiply_fusion) | copy-start | bytes 3145732
  112.8 2.5 copy-start.22
  115.3 9.1 %copy-start.3 = (bf16[1024,2048]{1,0:T(8,128)(2,1)S(1)}, bf16[1024,2048]{1,0:T(8,128)(2,1)}, u32[]{:S(2)}) copy-start(bf16[1024,2048]{1,0:T(8,128)(2,1)} %reshape.134) | copy-start | bytes 12582916
  120.7 2.8 copy-start.6
  120.7 3.7 copy-start.36
  125.8 2.3 copy-start.48
  132.1 1.4 copy-start.19
  133.5 15.6 %copy-start.39 = (f32[256,2,4]{2,1,0:T(2,128)}, f32[256,2,4]{2,1,0:T(2,128)S(1)}, u32[]{:S(2)}) copy-start(f32[256,2,4]{2,1,0:T(2,128)S(1)} %copy.597) | copy-start | bytes 24580
  149.1 1.4 copy-start.15
  150.5 2.5 copy-start.4
  150.5 2.5 copy-start.37
  157.2 11.8 %copy-start.34 = (f32[256,2,1,1]{3,2,1,0:T(1,128)S(1)}, f32[256,2,1,1]{3,2,1,0:T(1,128)}, u32[]{:S(2)}) copy-start(f32[256,2,1,1]{3,2,1,0:T(1,128)} %slice.141) | copy-start | bytes 6148
  170.8 7.6 %copy-start.8 = (f32[256,2,1,160]{3,2,1,0:T(1,128)}, f32[256,2,1,160]{3,2,1,0:T(1,128)S(1)}, u32[]{:S(2)}) copy-start(f32[256,2,1,160]{3,2,1,0:T(1,128)S(1)} %copy.650) | copy-start | bytes 983044
  170.8 8.9 %copy-start.29 = (f32[256,2,1,160]{3,2,1,0:T(1,128)S(1)}, f32[256,2,1,160]{3,2,1,0:T(1,128)}, u32[]{:S(2)}) copy-start(f32[256,2,1,160]{3,2,1,0:T(1,128)} %get-tuple-element.43) | copy-start | bytes 983044
  178.4 3.5 copy-start.33
  182.9 6.0 copy-start.7
  204.8 3.2 copy-start.23
  205.6 4.3 copy-start.28
  210.3 5.5 copy-start.27
  216.3 4.5 copy-start.9
  239.3 6.8 copy-start.10
  239.3 6.9 copy-start.11
  239.3 6.9 copy-start.12
  239.3 6.9 copy-start.13
  257.3 16.9 %copy-start.16 = (f32[256,2,4,128]{3,2,1,0:T(4,128)S(1)}, f32[256,2,4,128]{3,2,1,0:T(4,128)}, u32[]{:S(2)}) copy-start(f32[256,2,4,128]{3,2,1,0:T(4,128)} %copy-done.14) | copy-start | bytes 3145732
  257.4 16.9 %copy-start.18 = (f32[256,2,4,128]{3,2,1,0:T(4,128)S(1)}, f32[256,2,4,128]{3,2,1,0:T(4,128)}, u32[]{:S(2)}) copy-start(f32[256,2,4,128]{3,2,1,0:T(4,128)} %copy-done.17) | copy-start | bytes 3145732
  257.4 16.9 %copy-start.20 = (f32[256,4,2,128]{3,2,1,0:T(2,128)S(1)}, f32[256,4,2,128]{3,2,1,0:T(2,128)}, u32[]{:S(2)}) copy-start(f32[256,4,2,128]{3,2,1,0:T(2,128)} %copy-done.19) | copy-start | bytes 3145732
  257.4 16.9 %copy-start.25 = (f32[256,2,8,8]{3,2,1,0:T(8,128)S(1)}, f32[256,2,8,8]{3,2,1,0:T(8,128)}, u32[]{:S(2)}) copy-start(f32[256,2,8,8]{3,2,1,0:T(8,128)} %broadcast_subtract_fusion) | copy-start | bytes 393220
  257.4 16.9 %copy-start.35 = (f32[256,4,8]{2,1,0:T(4,128)S(1)}, f32[256,4,8]{2,1,0:T(4,128)}, u32[]{:S(2)}) copy-start(f32[256,4,8]{2,1,0:T(4,128)} %copy.617) | copy-start | bytes 98308
  257.4 16.9 %copy-start.40 = (f32[256,2,4]{2,1,0:T(2,128)S(1)}, f32[256,2,4]{2,1,0:T(2,128)}, u32[]{:S(2)}) copy-start(f32[256,2,4]{2,1,0:T(2,128)} %copy-done.39) | copy-start | bytes 24580
  278.6 4.6 copy-start.24
  283.2 9.3 %copy-start.38 = (bf16[2,32,2048]{2,1,0:T(8,128)(2,1)S(1)}, bf16[2,32,2048]{2,1,0:T(8,128)(2,1)}, u32[]{:S(2)}) copy-start(bf16[2,32,2048]{2,1,0:T(8,128)(2,1)} %param.31) | copy-start | bytes 786436
  297.1 424.0 %all-reduce.7.cloned.1.call-start = ((), (), s32[]{:S(2)}) async-start(), calls=%async_computation.2 | async-start | bytes 16777216 | tf_op jit(solution)/shard_map/psum | solution.py:218
  721.1 6.3 copy-start.1
  (5 other events, 4.6 us)
Sparse Core Ops, SparseCore 0:
  10.9 65.0 all-gather.1
  297.3 269.3 all-reduce.4
  569.1 151.9 all-reduce.6
